TPU v7x, 256 devices: a 8x8x2 block of a 8x8x16 slice. The times are simulated.
256 devices in a mesh: grp: 2 (over z), ep: 64 (over y, x), tp: 2 (over core).
Axes of the slice: x: 8, y: 8, z: 2, core: 2. Of those that a mesh axis runs over, the one named last changes fastest.
The devices are a block of a 8x8x16 slice.
Arguments:
- tokens: bfloat16 [4096, 2048], P(('grp', 'ep')), parts along dimension 0, may hold values from -6 to 6
- in_gain: bfloat16 [2048], replicated, may hold values from 0.099609375 to 1.8984375
- route_expert: int32 [4096, 6], P(('grp', 'ep')), parts along dimension 0, may hold values from 0 to 63, all different within a row; in each aligned block of 32 rows (0 to 31, 32 to 63, ...) at most 4 rows name the same one
- route_weight: float32 [4096, 6], P(('grp', 'ep')), parts along dimension 0, may hold values from 0.05 to 1
- gate_weight: bfloat16 [64, 2048, 768], P('ep', None, 'tp'), may hold values from -0.125 to 0.125
- up_weight: bfloat16 [64, 2048, 768], P('ep', None, 'tp'), may hold values from -0.125 to 0.125
- down_weight: bfloat16 [64, 768, 2048], P('ep', 'tp'), may hold values from -1 to 1
- shared_gate: bfloat16 [2048, 768], P(None, 'tp'), may hold values from -0.125 to 0.125
- shared_up: bfloat16 [2048, 768], P(None, 'tp'), may hold values from -0.125 to 0.125
- shared_down: bfloat16 [768, 2048], P('tp'), may hold values from -1 to 1
- out_gain: bfloat16 [2048], P('tp'), may hold values from 0.099609375 to 1.8984375
Outputs:
- mixed: bfloat16 [4096, 2048], P(('grp', 'ep'), 'tp'), parts along dimension 0
There are 2 independent parts, one for each index of `grp`. A program takes and returns all parts, laid end to end along the dimension named above; an argument that names none is the same for every part. Nothing has to cross between parts.
Inputs may be any that keep to these rules, and one draw needn't show every extreme that they name: `route_expert`: each row names 6 different experts. Among the rows of one device no expert is named more than 4 times, a bound that some block reaches.
All inputs are finite; a program needn't handle non-finite values.
Results may differ from a plain program's by a relative error of at most 0.0077.
Values may be sent and summed in bfloat16 or wider, within the bound.
A program may use at most 64 MiB of HBM per device.

v0:
```python
import jax
import jax.numpy as jnp
from jax import lax
from jax.sharding import PartitionSpec as P

EPSILON = 1e-06


def laid_out(blocks, dim):
    shape = list(blocks.shape[1:])
    shape[dim] *= blocks.shape[0]
    return jnp.moveaxis(blocks, 0, dim).reshape(shape)


def from_everyone(array, axis):
    devices = lax.axis_size(axis)
    return lax.all_to_all(
        jnp.broadcast_to(array[None], (devices, *array.shape)), axis, 0, 0, tiled=True
    )


def collect(array, axis, dim):
    return laid_out(from_everyone(array, axis), dim)


def in_blocks(array, dim, devices):
    before, after = (array.shape[:dim], array.shape[dim + 1 :])
    return jnp.moveaxis(array.reshape(*before, devices, -1, *after), dim, 0)


def sent_and_summed(array, axis, dim):
    devices = lax.axis_size(axis)
    blocks = lax.all_to_all(in_blocks(array, dim, devices), axis, 0, 0, tiled=True)
    return jnp.sum(blocks.astype(jnp.float32), axis=0)


def gathered_total(array, axis):
    return lax.all_gather(array, axis).sum(0)


def normalize(values, gain_vector):
    floats = values.astype(jnp.float32)
    scaled = floats * lax.rsqrt(jnp.mean(floats * floats, axis=-1, keepdims=True) + EPSILON)
    return (scaled * gain_vector.astype(jnp.float32)).astype(jnp.bfloat16)


def swiglu_hidden(inputs, gate_here, up_here):
    gate_value = jnp.dot(inputs, gate_here, preferred_element_type=jnp.float32)
    upward = jnp.dot(inputs, up_here, preferred_element_type=jnp.float32)
    return (jax.nn.silu(gate_value) * upward).astype(jnp.bfloat16)


def slot_tables(routes_here, experts, capacity):
    picked_count = routes_here.shape[0] * routes_here.shape[1]
    flattened = routes_here.reshape(picked_count)
    onehot = (flattened[:, None] == jnp.arange(experts, dtype=jnp.int32)[None, :]).astype(jnp.int32)
    earlier = jnp.cumsum(onehot, axis=0) - onehot
    ranked = jnp.sum(earlier * onehot, axis=1)
    slot_index = flattened * capacity + ranked
    source_token = jnp.arange(picked_count, dtype=jnp.int32) // routes_here.shape[1]
    matches = slot_index[None, :] == jnp.arange(experts * capacity, dtype=jnp.int32)[:, None]
    filled = jnp.any(matches, axis=1)
    slot_owner = jnp.sum(jnp.where(matches, source_token[None, :], 0), axis=1)
    return (slot_index, filled, slot_owner)


def body(
    tokens,
    in_gain,
    route_expert,
    route_weight,
    gate_weight,
    up_weight,
    down_weight,
    shared_gate,
    shared_up,
    shared_down,
    out_gain,
):
    experts = lax.axis_size("ep")
    local_tokens, model_width = tokens.shape
    top_count = route_expert.shape[1]
    capacity = max(2, (local_tokens * top_count * 4 + 3 * experts - 1) // (3 * experts))
    normed = normalize(tokens, in_gain)
    slot_index, filled, slot_owner = slot_tables(route_expert, experts, capacity)
    outgoing = jnp.where(filled[:, None], normed[slot_owner], jnp.zeros((), jnp.bfloat16))
    outgoing = outgoing.reshape(experts, capacity, model_width)
    half_width = model_width // lax.axis_size("tp")
    own_half = lax.dynamic_slice_in_dim(outgoing, lax.axis_index("tp") * half_width, half_width, 2)
    arrived = lax.all_to_all(own_half, "ep", split_axis=0, concat_axis=0, tiled=True)
    arrived = collect(arrived, "tp", 2)
    expert_rows = arrived.reshape(experts * capacity, model_width)
    expert_part = jnp.dot(
        swiglu_hidden(expert_rows, gate_weight[0], up_weight[0]),
        down_weight[0],
        preferred_element_type=jnp.float32,
    )
    shared_part = jnp.dot(
        swiglu_hidden(normed, shared_gate, shared_up),
        shared_down,
        preferred_element_type=jnp.float32,
    )
    summed = sent_and_summed(
        jnp.concatenate([expert_part, shared_part], axis=0).astype(jnp.bfloat16), "tp", 1
    )
    rounded = summed.astype(jnp.bfloat16)
    result_rows = rounded[: experts * capacity].reshape(experts, capacity, rounded.shape[1])
    shared_rows = rounded[experts * capacity :].astype(jnp.float32)
    returned = lax.all_to_all(result_rows, "ep", split_axis=0, concat_axis=0, tiled=True)
    returned = returned.reshape(experts * capacity, rounded.shape[1])
    picked = (
        returned[slot_index].astype(jnp.float32)
        * route_weight.reshape(local_tokens * top_count)[:, None]
    )
    combined = shared_rows + jnp.sum(
        picked.reshape(local_tokens, top_count, rounded.shape[1]), axis=1
    )
    squares = gathered_total(jnp.sum(combined * combined, axis=1), "tp")
    scaled = combined * lax.rsqrt(squares / model_width + EPSILON)[:, None]
    return (scaled * out_gain.astype(jnp.float32)).astype(jnp.bfloat16)


def solution(mesh):
    return jax.shard_map(
        body,
        mesh=mesh,
        in_specs=(
            P(("grp", "ep"), None),
            P(),
            P(("grp", "ep"), None),
            P(("grp", "ep"), None),
            P("ep", None, "tp"),
            P("ep", None, "tp"),
            P("ep", "tp", None),
            P(None, "tp"),
            P(None, "tp"),
            P("tp", None),
            P("tp"),
        ),
        out_specs=P(("grp", "ep"), "tp"),
        check_vma=False,
    )
```

profile of v0, /device:TPU:513, one launch (start us, length us, event | category | flops | bytes accessed | tf_op | source)
XLA Modules:
  0.0 102.2 jit_solution(11588395061193541111)
XLA Ops:
  0.0 0.9 copy.29
  0.9 0.1 reshape.122
  1.0 0.6 reduce-window.6
  1.6 0.2 slice_reduce_fusion
  1.9 0.1 bitcast_bitcast_fusion
  2.0 0.1 fusion.25
  2.1 0.1 select_reduce_fusion
  2.3 0.7 convert_element_type.41
  3.0 1.0 %fusion.21 = f32[32]{0:T(128)S(1)} fusion(bf16[32,2048]{1,0:T(8,128)(2,1)} %param.11), kind=kLoop, calls=%fused_computation.23 | loop fusion | flops 196576 | bytes 131200 | tf_op jit(solution)/shard_map/reduce_sum | solution.py:43
  4.0 1.0 fusion.23
  5.0 1.4 %gather_fusion = bf16[256,2048]{1,0:T(8,128)(2,1)S(1)} fusion(bf16[32,2048]{1,0:T(8,128)(2,1)S(1)} %fusion.23, s32[1024]{0:T(1024)S(1)} %pad_clamp_fusion.1), kind=kCustom, calls=%fused_computation | custom fusion | bytes 2098176 | tf_op jit(solution)/shard_map/gather | solution.py:86
  6.4 1.2 %gather.9 = bf16[64,4,2048]{2,1,0:T(4,128)(2,1)} reshape(bf16[256,2048]{1,0:T(8,128)(2,1)S(1)} %gather_fusion) | data formatting | bytes 2097152 | tf_op jit(solution)/shard_map/gather | solution.py:86
  7.6 0.1 broadcast_in_dim.28
  7.8 2.2 %dynamic-slice_select_fusion = bf16[64,4,1024]{2,1,0:T(4,128)(2,1)} fusion(bf16[64,4,2048]{2,1,0:T(4,128)(2,1)} %gather.9, s32[]{:T(128)S(6)} %select_n.45, pred[64,4]{1,0:T(8,128)(4,1)S(1)} %broadcast_in_dim.28), kind=kLoop, calls=%fused_computation.15 | loop fusion | flops 262144 | bytes 1048836 | tf_op jit(solution)/shard_map/jit(_where)/select_n | solution.py:86
  9.9 21.8 %all-to-all-start = ((bf16[64,4,1024]{2,1,0:T(4,128)(2,1)}), bf16[64,4,1024]{2,1,0:T(4,128)(2,1)S(1)}, u32[]{:S(2)}, u32[]{:S(2)}) async-start(bf16[64,4,1024]{2,1,0:T(4,128)(2,1)} %dynamic-slice_select_fusion), calls=%async_computation | async-start | bytes 1048576 | tf_op jit(solution)/shard_map/all_to_all | solution.py:90
  31.7 2.6 %copy.37 = bf16[2048,384]{1,0:T(8,128)(2,1)} copy(bf16[2048,384]{0,1:T(8,128)(2,1)} %bitcast.61) | data formatting | bytes 3145728 | tf_op jit(solution)/shard_map/dot_general | solution.py:93
  34.4 1.7 %fusion.36 = f32[32,384]{1,0:T(8,128)S(1)} fusion(bf16[32,2048]{1,0:T(8,128)(2,1)S(1)} %fusion.23, bf16[2048,384]{1,0:T(8,128)(2,1)} %param.18), kind=kOutput, calls=%fused_computation.64 | convolution fusion | flops 50331648 | bytes 1753088 | tf_op jit(solution)/shard_map/dot_general | solution.py:48
  36.1 2.6 %convolution_convert_fusion = bf16[32,2048]{1,0:T(8,128)(2,1)S(1)} fusion(bf16[384,2048]{1,0:T(8,128)(2,1)} %param.20, bf16[32,2048]{1,0:T(8,128)(2,1)S(1)} %fusion.23, bf16[2048,384]{1,0:T(8,128)(2,1)} %param.19, f32[32,384]{1,0:T(8,128)S(1)} %fusion.36), kind=kOutput, calls=%fused_computation.2 | convolution fusion | flops 100802560 | bytes 3457024 | tf_op jit(solution)/shard_map/dot_general | solution.py:98
  38.8 6.2 %all-to-all-done = bf16[64,4,1024]{2,1,0:T(4,128)(2,1)S(1)} async-done(((bf16[64,4,1024]{2,1,0:T(4,128)(2,1)}), bf16[64,4,1024]{2,1,0:T(4,128)(2,1)S(1)}, u32[]{:S(2)}, u32[]{:S(2)}) %all-to-all-start) | async-done | bytes 524320 | tf_op jit(solution)/shard_map/all_to_all | solution.py:90
  44.9 0.3 broadcast_in_dim.48
  45.2 10.5 %all_to_all.20 = bf16[2,64,4,1024]{3,2,1,0:T(4,128)(2,1)S(1)} all-to-all(bf16[2,64,4,1024]{3,2,1,0:T(4,128)(2,1)S(1)} %broadcast_in_dim.48), channel_id=1, replica_groups=mesh['grp'=2,'ep'=64,'tp'=2] {'tp'}, dimensions={0} | all-to-all | bytes 2097152 | tf_op jit(solution)/shard_map/all_to_all | solution.py:17
  55.7 1.1 %copy.32 = bf16[64,4,2,1024]{3,2,1,0:T(2,128)(2,1)S(1)} copy(bf16[64,4,2,1024]{3,1,0,2:T(4,128)(2,1)S(1)} %bitcast.59) | data formatting | bytes 2097152 | tf_op jit(solution)/shard_map/transpose | solution.py:12
  56.8 0.3 copy.41
  57.1 1.1 %copy-done.1 = bf16[1,2048,384]{2,1,0:T(8,128)(2,1)S(1)} copy-done((bf16[1,2048,384]{2,1,0:T(8,128)(2,1)S(1)}, bf16[1,2048,384]{2,1,0:T(8,128)(2,1)}, u32[]{:S(2)}) %copy-start.1) | copy-done | bytes 1572888
  58.2 0.7 fusion.2
  58.9 3.7 %convolution_convert_fusion.1 = bf16[256,2,1024]{2,0,1:T(8,128)(2,1)} fusion(bf16[2,1024,384]{2,1,0:T(8,128)(2,1)} %bitcast.62, bf16[256,2048]{1,0:T(8,128)(2,1)S(1)} %bitcast.58, bf16[1,2048,384]{2,1,0:T(8,128)(2,1)S(1)} %copy-done, f32[256,384]{1,0:T(8,128)S(1)} %fusion.2), kind=kOutput, calls=%fused_computation.7 | convolution fusion | flops 806420480 | bytes 5636096 | tf_op jit(solution)/shard_map/dot_general | solution.py:93
  62.6 1.3 %maximum_bitcast_fusion = bf16[2,288,1024]{2,1,0:T(8,128)(2,1)S(1)} fusion(bf16[32,2,1024]{2,0,1:T(8,128)(2,1)S(1)} %bitcast.63, bf16[256,2,1024]{2,0,1:T(8,128)(2,1)} %convolution_convert_fusion.1), kind=kLoop, calls=%fused_computation.9 | loop fusion | flops 2359296 | bytes 2359296 | tf_op jit(solution)/shard_map/transpose | solution.py:28
  64.0 4.7 %all_to_all.21 = bf16[2,288,1024]{2,1,0:T(8,128)(2,1)S(1)} all-to-all(bf16[2,288,1024]{2,1,0:T(8,128)(2,1)S(1)} %maximum_bitcast_fusion), channel_id=1, replica_groups=mesh['grp'=2,'ep'=64,'tp'=2] {'tp'}, dimensions={0} | all-to-all | bytes 2359296 | tf_op jit(solution)/shard_map/all_to_all | solution.py:33
  68.7 0.3 reduce_sum.74
  69.0 0.0 copy-start.3
  69.0 0.0 copy-start.4
  69.0 0.0 copy-start.5
  69.0 1.0 reshape.125
  70.0 6.5 %all-to-all-start.3 = ((bf16[64,4,1024]{2,1,0:T(4,128)(2,1)}), bf16[64,4,1024]{2,1,0:T(4,128)(2,1)S(1)}, u32[]{:S(2)}, u32[]{:S(2)}) async-start(bf16[64,4,1024]{2,1,0:T(4,128)(2,1)} %reshape.125), calls=%async_computation.3 | async-start | bytes 1048576 | tf_op jit(solution)/shard_map/all_to_all | solution.py:109
  76.5 0.1 copy.35
  76.6 0.1 mul.106
  76.7 0.1 copy.36
  76.8 0.6 dynamic-slice
  78.1 14.7 %all-to-all-done.3 = bf16[64,4,1024]{2,1,0:T(4,128)(2,1)S(1)} async-done(((bf16[64,4,1024]{2,1,0:T(4,128)(2,1)}), bf16[64,4,1024]{2,1,0:T(4,128)(2,1)S(1)}, u32[]{:S(2)}, u32[]{:S(2)}) %all-to-all-start.3) | async-done | bytes 524320 | tf_op jit(solution)/shard_map/all_to_all | solution.py:109
  92.8 0.1 reshape.126
  93.0 1.8 %gather_fusion.1 = bf16[192,1024]{1,0:T(8,128)(2,1)} fusion(bf16[256,1024]{1,0:T(8,128)(2,1)S(1)} %reshape.126, s32[1024]{0:T(1024)S(1)} %pad_clamp_fusion), kind=kCustom, calls=%fused_computation.1 | custom fusion | bytes 787200 | tf_op jit(solution)/shard_map/gather | solution.py:112
  94.7 1.1 %reshape.128 = f32[32,6,1024]{2,1,0:T(8,128)S(1)} reshape(bf16[192,1024]{1,0:T(8,128)(2,1)} %gather_fusion.1) | data formatting | bytes 1179648 | tf_op jit(solution)/shard_map/convert_element_type | solution.py:112
  95.8 0.4 multiply_reduce_fusion
  96.2 0.1 multiply_reduce_fusion.1
  96.3 0.2 dynamic-update-slice
  96.6 4.8 %all-reduce.1 = f32[64]{0:T(128)S(1)} all-reduce(f32[64]{0:T(128)S(1)} %dynamic-update-slice), channel_id=2, replica_groups=mesh['grp'=2,'ep'=64,'tp'=2] {'tp'}, use_global_device_ids=true, to_apply=%add.1 | all-reduce | flops 64 | bytes 512
  101.4 0.1 reshape.145
  101.5 0.7 multiply_convert_fusion
  (26 shorter events, 0.3 us)
Async XLA Ops:
  0.0 58.9 %copy-start = (bf16[1,2048,384]{2,1,0:T(8,128)(2,1)S(1)}, bf16[1,2048,384]{2,1,0:T(8,128)(2,1)}, u32[]{:S(2)}) copy-start(bf16[1,2048,384]{2,1,0:T(8,128)(2,1)} %param.16) | copy-start | bytes 4718596
  9.9 35.0 %all-to-all-start = ((bf16[64,4,1024]{2,1,0:T(4,128)(2,1)}), bf16[64,4,1024]{2,1,0:T(4,128)(2,1)S(1)}, u32[]{:S(2)}, u32[]{:S(2)}) async-start(bf16[64,4,1024]{2,1,0:T(4,128)(2,1)} %dynamic-slice_select_fusion), calls=%async_computation | async-start | bytes 1048576 | tf_op jit(solution)/shard_map/all_to_all | solution.py:90
  56.8 1.4 %copy-start.1 = (bf16[1,2048,384]{2,1,0:T(8,128)(2,1)S(1)}, bf16[1,2048,384]{2,1,0:T(8,128)(2,1)}, u32[]{:S(2)}) copy-start(bf16[1,2048,384]{2,1,0:T(8,128)(2,1)} %param.15) | copy-start | bytes 4718596
  68.9 7.6 %copy-start.2 = (s32[32,6]{0,1:T(8,128)S(1)}, s32[32,6]{0,1:T(8,128)}, u32[]{:S(2)}) copy-start(s32[32,6]{0,1:T(8,128)} %param.13) | copy-start | bytes 2308
  69.0 7.8 %copy-start.3 = (f32[32,6]{0,1:T(8,128)S(1)}, f32[32,6]{0,1:T(8,128)}, u32[]{:S(2)}) copy-start(f32[32,6]{0,1:T(8,128)} %param.14) | copy-start | bytes 2308
  69.0 7.9 %copy-start.4 = (bf16[1024]{0:T(1024)(128)(2,1)S(1)}, bf16[1024]{0:T(1024)(128)(2,1)}, u32[]{:S(2)}) copy-start(bf16[1024]{0:T(1024)(128)(2,1)} %param.21) | copy-start | bytes 6148
  69.0 7.9 %copy-start.5 = (u32[256]{0:T(256)S(1)}, u32[256]{0:T(256)}, u32[]{:S(2)}) copy-start(u32[256]{0:T(256)} %constant.63) | copy-start | bytes 3076
  70.0 22.8 %all-to-all-start.3 = ((bf16[64,4,1024]{2,1,0:T(4,128)(2,1)}), bf16[64,4,1024]{2,1,0:T(4,128)(2,1)S(1)}, u32[]{:S(2)}, u32[]{:S(2)}) async-start(bf16[64,4,1024]{2,1,0:T(4,128)(2,1)} %reshape.125), calls=%async_computation.3 | async-start | bytes 1048576 | tf_op jit(solution)/shard_map/all_to_all | solution.py:109
where the time goes:
time: 103 us; the launch traced here: 102 us
  starting transfers between devices  28.3 us (27%)
  waiting for transfers between devices  20.9 us (20%)
  blocking collectives  20 us (19%)
  local copies, waits for them, and re-layouts  14.5 us (14%)
  other arithmetic  8.86 us (9%)
  matrix products  8.8 us (9%)
    all_to_all x1, starting transfers between devices, body(): lax.all_to_all(own_half, 'ep', split_axis=0, concat_axis=0, tiled=True)  21.8 us
    all_to_all x1, waiting for transfers between devices, body(): lax.all_to_all(result_rows, 'ep', split_axis=0, concat_axis=0, tiled=True)  14.7 us
    all_to_all x1, blocking collectives, from_everyone(): lax.all_to_all(jnp.broadcast_to(array[None], (devices, *array.shape)), ax...  10.5 us
    all_to_all x1, starting transfers between devices, body(): lax.all_to_all(result_rows, 'ep', split_axis=0, concat_axis=0, tiled=True)  6.49 us
    all_to_all x1, waiting for transfers between devices, body(): lax.all_to_all(own_half, 'ep', split_axis=0, concat_axis=0, tiled=True)  6.16 us
    unnamed x1, blocking collectives  4.82 us
    all_to_all x1, blocking collectives, sent_and_summed(): lax.all_to_all(in_blocks(array, dim, devices), axis, 0, 0, tiled=True)  4.7 us
    dot_general x1, matrix products, body(): jnp.dot(swiglu_hidden(expert_rows, gate_weight[0], up_weight[0]), down_we...  3.71 us
  transfers between devices with their start and end apart: 2, of which 2 were waited for; matrix products, arithmetic and copies ran while one was open for 8% of the time, Pallas kernels for 0%

commit v1 on v0

v1 whole, which is shorter than its diff:
```python
import functools
import math

import jax
import jax.numpy as jnp
from jax import lax
from jax.experimental import pallas as pl
from jax.experimental.pallas import tpu as pltpu
from jax.sharding import PartitionSpec as P

EPSILON = 1e-06
BF16 = jnp.bfloat16
F32 = jnp.float32
LANES = 128
MESH = pl.DeviceIdType.MESH


def far_first(side):
    def reach(step):
        return min(step, side - step)

    offsets = [(dx, dy) for dy in range(side) for dx in range(side) if dx or dy]
    return sorted(offsets, key=lambda o: -(reach(o[0]) + reach(o[1])))


def dot(a, b):
    return jnp.dot(a, b, preferred_element_type=F32)


def iota(shape, dim):
    return lax.broadcasted_iota(jnp.int32, shape, dim)


def one_hot_to_rows(blocks, per_row):
    size = blocks * per_row
    row, col = iota((size, size), 0), iota((size, size), 1)
    return (col == (row % blocks) * per_row + row // blocks).astype(F32).astype(BF16)


def one_hot_to_blocks(blocks, per_row):
    size = blocks * per_row
    row, col = iota((size, size), 0), iota((size, size), 1)
    return (col == (row % per_row) * blocks + row // per_row).astype(F32).astype(BF16)


def kernel(
    experts, cores, slots,
    tokens_hbm, in_gain_hbm, route_hbm, weight_hbm, gate_hbm, up_hbm, down_hbm, sgate_hbm, sup_hbm, sdown_hbm, out_gain_hbm,
    out_ref,
    tokens, in_gain, route, weight, out_gain, gate, up, down, sgate, sup, sdown,
    normed, tx, rx, rows, tx2, rx2, picks, shared_send, shared_recv, shared_half, sq_send, sq_recv,
    small_sem, weight_sem, push_send, push_recv, send_sem, recv_sem, send2_sem, recv2_sem, pair_send, pair_recv, ready_sem,
):
    ep, c = lax.axis_index("ep"), lax.axis_index("tp")
    other = 1 - c
    side = math.isqrt(experts)
    here_x, here_y = lax.rem(ep, side), lax.div(ep, side)
    local_tokens, width = tokens.shape
    half = width // cores
    chunks = slots // cores
    wide = width // LANES
    thin = half // LANES
    order = far_first(side)

    def peer(offset):
        return lax.rem(here_y + offset[1], side) * side + lax.rem(here_x + offset[0], side)

    small = [
        pltpu.make_async_copy(src, dst, small_sem.at[i])
        for i, (src, dst) in enumerate(
            [(route_hbm, route), (tokens_hbm, tokens), (in_gain_hbm, in_gain), (weight_hbm, weight), (out_gain_hbm, out_gain)]
        )
    ]
    for copy in small:
        copy.start()
    barrier = pltpu.get_barrier_semaphore()
    for offset in order:
        pl.semaphore_signal(barrier, inc=1, device_id={"ep": peer(offset)}, device_id_type=MESH)
    pl.semaphore_signal(barrier, inc=1, device_id={"tp": other}, device_id_type=MESH)
    loads = [
        pltpu.make_async_copy(src, dst, weight_sem.at[i])
        for i, (src, dst) in enumerate(
            [
                (sgate_hbm, sgate), (sup_hbm, sup), (sdown_hbm, sdown),
                (gate_hbm.at[0], gate.at[0]), (up_hbm.at[0], up.at[0]), (down_hbm.at[0], down.at[0]),
            ]
        )
    ]
    for copy in loads:
        copy.start()

    small[0].wait()
    names = route[...]
    expert_lane = iota((local_tokens, LANES), 1)
    hits = [names[:, k : k + 1] == expert_lane for k in range(names.shape[1])]
    chosen = functools.reduce(jnp.logical_or, hits)
    chosen_f = chosen.astype(F32)
    lower = (iota((local_tokens, local_tokens), 0) > iota((local_tokens, local_tokens), 1)).astype(F32).astype(BF16)
    rank = jnp.where(chosen, dot(lower, chosen_f.astype(BF16)), -1.0)
    rank_b = rank.astype(BF16)
    eye = (iota((experts, LANES), 0) == iota((experts, LANES), 1)).astype(F32).astype(BF16)
    rank_t = lax.dot_general(eye, rank_b, (((1,), (1,)), ((), ())), preferred_element_type=F32)

    small[1].wait()
    small[2].wait()
    floats = tokens[...].astype(F32)
    scale = lax.rsqrt(jnp.mean(floats * floats, axis=1, keepdims=True) + EPSILON)
    normed[...] = (floats * scale * in_gain[...].astype(F32)).astype(BF16)

    to_blocks = one_hot_to_blocks(wide, wide)
    per_block = wide
    first_slot = (c * chunks).astype(F32)
    for j in range(chunks):
        pick = (rank_t == first_slot + j).astype(F32).astype(BF16)
        picked = dot(pick, normed[...]).astype(BF16)
        for b in range(experts // per_block):
            part = picked[b * per_block : (b + 1) * per_block]
            stacked = jnp.concatenate([part[:, q * LANES : (q + 1) * LANES] for q in range(wide)], axis=0)
            tx[j, pl.ds(b * per_block, per_block)] = (
                dot(to_blocks, stacked).astype(BF16).reshape(per_block, wide, LANES)
            )
        rx[j, ep] = tx[j, ep]

    pl.semaphore_wait(barrier, experts)
    pl.semaphore_signal(ready_sem, inc=1, device_id={"tp": other}, device_id_type=MESH)

    def dispatch(j, offset):
        to = peer(offset)
        return pltpu.make_async_remote_copy(
            src_ref=tx.at[j, to], dst_ref=rx.at[j, ep], send_sem=send_sem.at[j], recv_sem=recv_sem.at[j],
            device_id={"ep": to}, device_id_type=MESH,
        )

    for j in range(chunks):
        for offset in order:
            dispatch(j, offset).start()
    pushes = [
        pltpu.make_async_remote_copy(
            src_ref=src.at[0], dst_ref=dst.at[1], send_sem=push_send.at[i], recv_sem=push_recv.at[i],
            device_id={"tp": other}, device_id_type=MESH,
        )
        for i, (src, dst) in enumerate([(gate_hbm, gate), (up_hbm, up), (down_hbm, down)])
    ]
    for copy in pushes:
        copy.start()

    def swiglu(inputs, pairs):
        hidden = []
        for gate_here, up_here in pairs:
            gate_value = dot(inputs, gate_here)
            upward = dot(inputs, up_here)
            hidden.append((jax.nn.silu(gate_value) * upward).astype(BF16))
        return hidden

    for copy in loads[:3]:
        copy.wait()
    (hidden,) = swiglu(normed[...], [(sgate[...], sup[...])])
    shared_part = dot(hidden, sdown[...]).astype(BF16)
    for side_of in range(cores):
        shared_send[side_of] = shared_part[:, side_of * half : (side_of + 1) * half]
    pair = pltpu.make_async_remote_copy(
        src_ref=shared_send.at[other], dst_ref=shared_recv, send_sem=pair_send.at[0], recv_sem=pair_recv.at[0],
        device_id={"tp": other}, device_id_type=MESH,
    )
    pair.start()

    small[3].wait()
    small[4].wait()
    weights = weight[...]
    weight_at = functools.reduce(
        jnp.add, [jnp.where(hit, weights[:, k : k + 1], 0.0) for k, hit in enumerate(hits)]
    )
    high = weight_at.astype(BF16)
    low = (weight_at - high.astype(F32)).astype(BF16)
    columns = experts * cores * thin
    col = iota((LANES, columns), 1)
    expand = (iota((LANES, columns), 0) == col // (cores * thin)).astype(F32).astype(BF16)
    spread = dot(jnp.concatenate([high, low, rank_b], axis=0), expand)
    col = iota((local_tokens, columns), 1)
    slot_base = ((col // thin) % cores * chunks).astype(F32)
    q_col = col % thin
    for j in range(chunks):
        here = spread[2 * local_tokens :] == slot_base + j
        for part in range(2):
            value = jnp.where(here, spread[part * local_tokens : (part + 1) * local_tokens], 0.0)
            for q in range(thin):
                picks[j, pl.ds((part * thin + q) * local_tokens, local_tokens)] = jnp.where(
                    q_col == q, value, 0.0
                ).astype(BF16)

    pair.wait()
    for q in range(thin):
        lanes = slice(q * LANES, (q + 1) * LANES)
        total = shared_send[c][:, lanes].astype(F32) + shared_recv[:, lanes].astype(F32)
        shared_half[pl.ds(q * local_tokens, local_tokens)] = total.astype(BF16).astype(F32)

    for copy in loads[3:]:
        copy.wait()
    for copy in pushes:
        copy.wait()
    pl.semaphore_wait(ready_sem, 1)

    to_rows = one_hot_to_rows(wide, wide)
    per_back = 2 * LANES // thin
    to_thin = one_hot_to_blocks(per_back, thin)

    def give_back(j, offset, core):
        to = peer(offset)
        return pltpu.make_async_remote_copy(
            src_ref=tx2.at[j, core, to], dst_ref=rx2.at[j, ep * cores + c], send_sem=send2_sem.at[j], recv_sem=recv2_sem.at[j],
            device_id={"ep": to, "tp": core}, device_id_type=MESH,
        )

    partner_back = []
    for j in range(chunks):
        arrived = rx.at[j, pl.ds(0, experts - 1)]
        pltpu.make_async_copy(arrived, arrived, recv_sem.at[j]).wait()
        for b in range(experts // per_block):
            block = rx[j, pl.ds(b * per_block, per_block)].reshape(per_block * wide, LANES)
            sorted_rows = dot(to_rows, block).astype(BF16)
            for q in range(wide):
                rows[pl.ds(b * per_block, per_block), q * LANES : (q + 1) * LANES] = sorted_rows[
                    q * per_block : (q + 1) * per_block
                ]
        hidden = swiglu(rows[...], [(gate[h], up[h]) for h in range(cores)])
        result = functools.reduce(jnp.add, [dot(hidden[h], down[h]) for h in range(cores)]).astype(BF16)
        for b in range(experts // per_back):
            part = result[b * per_back : (b + 1) * per_back]
            for core in range(cores):
                stacked = jnp.concatenate(
                    [part[:, core * half + q * LANES : core * half + (q + 1) * LANES] for q in range(thin)], axis=0
                )
                tx2[j, core, pl.ds(b * per_back, per_back)] = (
                    dot(to_thin, stacked).astype(BF16).reshape(per_back, thin, LANES)
                )
        for offset in order:
            for core in range(cores):
                give_back(j, offset, core).start()
        back = pltpu.make_async_remote_copy(
            src_ref=tx2.at[j, other, ep], dst_ref=rx2.at[j, ep * cores + c], send_sem=send2_sem.at[j], recv_sem=recv2_sem.at[j],
            device_id={"tp": other}, device_id_type=MESH,
        )
        back.start()
        rx2[j, ep * cores + c] = tx2[j, c, ep]

    total = shared_half[...]
    for j in range(chunks):
        arrived = rx2.at[j, pl.ds(0, experts * cores - 1)]
        pltpu.make_async_copy(arrived, arrived, recv2_sem.at[j]).wait()
        summed = dot(picks[j], rx2[j].reshape(experts * cores * thin, LANES))
        total = total + summed[: thin * local_tokens] + summed[thin * local_tokens :]
    squares = total * total
    mine = functools.reduce(jnp.add, [squares[q * local_tokens : (q + 1) * local_tokens] for q in range(thin)])
    mine = jnp.broadcast_to(jnp.sum(mine, axis=1, keepdims=True), (local_tokens, LANES))
    sq_send[...] = mine
    pair = pltpu.make_async_remote_copy(
        src_ref=sq_send, dst_ref=sq_recv, send_sem=pair_send.at[1], recv_sem=pair_recv.at[1],
        device_id={"tp": other}, device_id_type=MESH,
    )
    pair.start()
    for j in range(chunks):
        sent = tx.at[j, pl.ds(0, experts - 1)]
        pltpu.make_async_copy(sent, sent, send_sem.at[j]).wait()
        sent = rx2.at[j, pl.ds(0, experts * cores - 1)]
        pltpu.make_async_copy(sent, sent, send2_sem.at[j]).wait()
    pair.wait()
    scale = lax.rsqrt((mine + sq_recv[...]) / width + EPSILON)
    gain = out_gain[...].astype(F32)
    for q in range(thin):
        lanes = slice(q * LANES, (q + 1) * LANES)
        out_ref[:, lanes] = (total[q * local_tokens : (q + 1) * local_tokens] * scale * gain[:, lanes]).astype(BF16)


def body(tokens, in_gain, route_expert, route_weight, gate_weight, up_weight, down_weight, shared_gate, shared_up, shared_down, out_gain):
    experts, cores = lax.axis_size("ep"), lax.axis_size("tp")
    local_tokens, width = tokens.shape
    top_count = route_expert.shape[1]
    slots = max(2, (local_tokens * top_count * 4 + 3 * experts - 1) // (3 * experts))
    chunks = slots // cores
    half = width // cores
    wide, thin = width // LANES, half // LANES
    hidden = gate_weight.shape[2]
    any_spec = pl.BlockSpec(memory_space=pl.ANY)
    vmem, dma = pltpu.VMEM, pltpu.SemaphoreType.DMA
    scratch = [
        vmem((local_tokens, width), BF16), vmem((1, width), BF16), vmem((local_tokens, top_count), jnp.int32),
        vmem((local_tokens, top_count), F32), vmem((1, half), BF16),
        vmem((cores, width, hidden), BF16), vmem((cores, width, hidden), BF16), vmem((cores, hidden, width), BF16),
        vmem((width, hidden), BF16), vmem((width, hidden), BF16), vmem((hidden, width), BF16),
        vmem((local_tokens, width), BF16),
        vmem((chunks, experts, wide, LANES), BF16), vmem((chunks, experts, wide, LANES), BF16),
        vmem((experts, width), BF16),
        vmem((chunks, cores, experts, thin, LANES), BF16), vmem((chunks, experts * cores, thin, LANES), BF16),
        vmem((chunks, 2 * thin * local_tokens, experts * cores * thin), BF16),
        vmem((cores, local_tokens, half), BF16), vmem((local_tokens, half), BF16), vmem((thin * local_tokens, LANES), F32),
        vmem((local_tokens, LANES), F32), vmem((local_tokens, LANES), F32),
        dma((5,)), dma((6,)), dma((3,)), dma((3,)), dma((chunks,)), dma((chunks,)), dma((chunks,)), dma((chunks,)),
        dma((2,)), dma((2,)), pltpu.SemaphoreType.REGULAR,
    ]
    return pl.pallas_call(
        functools.partial(kernel, experts, cores, slots),
        out_shape=jax.ShapeDtypeStruct((local_tokens, half), BF16),
        in_specs=[any_spec] * 11,
        out_specs=pl.BlockSpec(memory_space=pltpu.VMEM),
        scratch_shapes=scratch,
        compiler_params=pltpu.CompilerParams(collective_id=0, has_side_effects=True, vmem_limit_bytes=60 * 1024 * 1024),
    )(
        tokens, in_gain.reshape(1, width), route_expert, route_weight, gate_weight, up_weight, down_weight,
        shared_gate, shared_up, shared_down, out_gain.reshape(1, half),
    )


def solution(mesh):
    return jax.shard_map(
        body,
        mesh=mesh,
        in_specs=(
            P(("grp", "ep"), None),
            P(),
            P(("grp", "ep"), None),
            P(("grp", "ep"), None),
            P("ep", None, "tp"),
            P("ep", None, "tp"),
            P("ep", "tp", None),
            P(None, "tp"),
            P(None, "tp"),
            P("tp", None),
            P("tp"),
        ),
        out_specs=P(("grp", "ep"), "tp"),
        check_vma=False,
    )
```

time: 103 us -> 61.8 us (0.60)
  Pallas kernels: 0 us -> 54.8 us
  starting transfers between devices: 28.3 us -> 0 us
  waiting for transfers between devices: 20.9 us -> 0 us
  blocking collectives: 20 us -> 0 us
  other arithmetic: 8.86 us -> 0 us
  matrix products: 8.8 us -> 0 us
  local copies, waits for them, and re-layouts: 14.5 us -> 6.78 us
    pallas_call x0 -> x1, Pallas kernels: none -> 54.8 us  [body(): pl.pallas_call(functools.partial(kernel, experts, cores, slots), out_shap...]
    all_to_all x2 -> x0, starting transfers between devices: 28.3 us -> none  [the longest x1 21.8 us: body(): lax.all_to_all(own_half, 'ep', split_axis=0, concat_axis=0, tiled=True)]
    all_to_all x2 -> x0, waiting for transfers between devices: 20.9 us -> none  [the longest x1 14.7 us: body(): lax.all_to_all(result_rows, 'ep', split_axis=0, concat_axis=0, tiled=True)]
    all_to_all x2 -> x0, blocking collectives: 15.2 us -> none  [the longest x1 10.5 us: from_everyone(): lax.all_to_all(jnp.broadcast_to(array[None], (devices, *array.shape)), ax...]
    dot_general x4 -> x0, matrix products: 8.8 us -> none  [the longest x1 3.71 us: body(): jnp.dot(swiglu_hidden(expert_rows, gate_weight[0], up_weight[0]), down_we...]
    unnamed x1 -> x0, blocking collectives: 4.82 us -> none
    gather x3 -> x0, local copies, waits for them, and re-layouts: 4.34 us -> none  [the longest x2 2.59 us: body(): normed[slot_owner]]
    dot_general x1 -> x0, local copies, waits for them, and re-layouts: 2.61 us -> none  [body(): jnp.dot(swiglu_hidden(expert_rows, gate_weight[0], up_weight[0]), down_we...]
  transfers between devices with their start and end apart: 2 -> 0, of which waited for: 2 -> 0; matrix products, arithmetic and copies ran while one was open for 8% -> 0% of each run, Pallas kernels for 0% -> 0%
where the time goes in v1:
time: 61.8 us; the launch traced here: 61.5 us
  Pallas kernels  54.8 us (89%)
  local copies, waits for them, and re-layouts  6.78 us (11%)
    pallas_call x1, Pallas kernels, body(): pl.pallas_call(functools.partial(kernel, experts, cores, slots), out_shap...  54.8 us
    unnamed x3, local copies, waits for them, and re-layouts  4.21 us
    reshape x1, local copies, waits for them, and re-layouts, body(): in_gain.reshape(1, width)  1.29 us
    reshape x1, local copies, waits for them, and re-layouts, body(): out_gain.reshape(1, half)  1.28 us

profile of v1, /device:TPU:513, one launch (start us, length us, event | category | flops | bytes accessed | tf_op | source)
XLA Modules:
  0.0 61.5 jit_solution(7769967555625997631)
XLA Ops:
  0.0 1.3 %reshape.7.out_gain_hbm = bf16[1,1024]{1,0:T(2,128)(2,1)} reshape(bf16[1024]{0:T(1024)(128)(2,1)} %param.21) | data formatting | bytes 4096 | tf_op jit(solution)/shard_map/reshape | solution.py:309
  1.3 1.3 %reshape.6.in_gain_hbm = bf16[1,2048]{1,0:T(2,128)(2,1)} reshape(bf16[2048]{0:T(1024)(128)(2,1)} %param.12) | data formatting | bytes 8192 | tf_op jit(solution)/shard_map/reshape | solution.py:308
  2.6 1.4 %copy.12.route_hbm = s32[32,6]{1,0:T(8,128)} copy(s32[32,6]{0,1:T(8,128)} %param.13) | data formatting | bytes 1536 | tf_op args[2]
  3.9 1.4 %copy.13.weight_hbm = f32[32,6]{1,0:T(8,128)} copy(f32[32,6]{0,1:T(8,128)} %param.14) | data formatting | bytes 1536 | tf_op args[3]
  5.3 54.8 %shard_map.109 = bf16[32,1024]{1,0:T(8,128)(2,1)} custom-call(bf16[32,2048]{1,0:T(8,128)(2,1)} %tokens_hbm.1, bf16[1,2048]{1,0:T(2,128)(2,1)} %reshape.6.in_gain_hbm, s32[32,6]{1,0:T(8,128)} %copy.12.route_hbm, f32[32,6]{1,0:T(8,128)} %copy.13.weight_hbm, bf16[1,2048,384]{2,1,0:T(8,128)(2,1)} %gate_hbm.1, bf16[1,2048,384]{2,1,0:T(8,128)(2,1)} %up_hbm.1, ...), custom_call_target="tpu_custom_call" | custom-call | tf_op jit(solution)/shard_map/pallas_call | solution.py:300
  60.1 1.5 %copy.15 = bf16[32,1024]{1,0:T(8,128)(2,1)} copy(bf16[32,1024]{1,0:T(8,128)(2,1)} %shard_map.109) | data formatting | bytes 131072

commit v2 on v1

--- a/solution.py
+++ b/solution.py
@@ -20,7 +20,9 @@
         return min(step, side - step)
 
     offsets = [(dx, dy) for dy in range(side) for dx in range(side) if dx or dy]
-    return sorted(offsets, key=lambda o: -(reach(o[0]) + reach(o[1])))
+    offsets = sorted(offsets, key=lambda o: -(reach(o[0]) + reach(o[1])))
+    straight = [o for o in offsets if not (o[0] and o[1])]
+    return straight, [o for o in offsets if o[0] and o[1]]
 
 
 def dot(a, b):
@@ -49,7 +51,7 @@
     out_ref,
     tokens, in_gain, route, weight, out_gain, gate, up, down, sgate, sup, sdown,
     normed, tx, rx, rows, tx2, rx2, picks, shared_send, shared_recv, shared_half, sq_send, sq_recv,
-    small_sem, weight_sem, push_send, push_recv, send_sem, recv_sem, send2_sem, recv2_sem, pair_send, pair_recv, ready_sem,
+    small_sem, weight_sem, push_send, push_recv, send_sem, recv_sem, send2_sem, recv2_sem, pair_send, pair_recv, pair_sem, lines_sem, planes_sem,
 ):
     ep, c = lax.axis_index("ep"), lax.axis_index("tp")
     other = 1 - c
@@ -60,7 +62,8 @@
     chunks = slots // cores
     wide = width // LANES
     thin = half // LANES
-    order = far_first(side)
+    straight, diagonal = far_first(side)
+    order = diagonal + straight
 
     def peer(offset):
         return lax.rem(here_y + offset[1], side) * side + lax.rem(here_x + offset[0], side)
@@ -74,9 +77,31 @@
     for copy in small:
         copy.start()
     barrier = pltpu.get_barrier_semaphore()
-    for offset in order:
-        pl.semaphore_signal(barrier, inc=1, device_id={"ep": peer(offset)}, device_id_type=MESH)
-    pl.semaphore_signal(barrier, inc=1, device_id={"tp": other}, device_id_type=MESH)
+
+    @pl.when(c == 0)
+    def _():
+        pl.semaphore_signal(barrier, inc=1, device_id={"tp": 1}, device_id_type=MESH)
+
+    @pl.when(c == 1)
+    def _():
+        pl.semaphore_wait(barrier, 1)
+        pl.semaphore_signal(pair_sem, inc=1, device_id={"tp": 0}, device_id_type=MESH)
+
+    @pl.when(c == 0)
+    def _():
+        pl.semaphore_wait(pair_sem, 1)
+        for offset in straight:
+            pl.semaphore_signal(barrier, inc=1, device_id={"ep": peer(offset)}, device_id_type=MESH)
+
+    pushes = [
+        pltpu.make_async_remote_copy(
+            src_ref=src.at[0], dst_ref=dst.at[1], send_sem=push_send.at[i], recv_sem=push_recv.at[i],
+            device_id={"tp": other}, device_id_type=MESH,
+        )
+        for i, (src, dst) in enumerate([(gate_hbm, gate), (up_hbm, up), (down_hbm, down)])
+    ]
+    for copy in pushes:
+        copy.start()
     loads = [
         pltpu.make_async_copy(src, dst, weight_sem.at[i])
         for i, (src, dst) in enumerate(
@@ -91,21 +116,20 @@
 
     small[0].wait()
     names = route[...]
-    expert_lane = iota((local_tokens, LANES), 1)
-    hits = [names[:, k : k + 1] == expert_lane for k in range(names.shape[1])]
+    expert_row = iota((experts, local_tokens), 0)
+    hits = [names[k : k + 1, :] == expert_row for k in range(names.shape[0])]
     chosen = functools.reduce(jnp.logical_or, hits)
-    chosen_f = chosen.astype(F32)
-    lower = (iota((local_tokens, local_tokens), 0) > iota((local_tokens, local_tokens), 1)).astype(F32).astype(BF16)
-    rank = jnp.where(chosen, dot(lower, chosen_f.astype(BF16)), -1.0)
-    rank_b = rank.astype(BF16)
-    eye = (iota((experts, LANES), 0) == iota((experts, LANES), 1)).astype(F32).astype(BF16)
-    rank_t = lax.dot_general(eye, rank_b, (((1,), (1,)), ((), ())), preferred_element_type=F32)
+    earlier = (iota((local_tokens, local_tokens), 0) < iota((local_tokens, local_tokens), 1)).astype(F32).astype(BF16)
+    rank_t = jnp.where(chosen, dot(chosen.astype(F32).astype(BF16), earlier), -1.0)
 
     small[1].wait()
     small[2].wait()
     floats = tokens[...].astype(F32)
     scale = lax.rsqrt(jnp.mean(floats * floats, axis=1, keepdims=True) + EPSILON)
-    normed[...] = (floats * scale * in_gain[...].astype(F32)).astype(BF16)
+    gains = in_gain[...].astype(F32)
+    for q in range(wide):
+        lanes = slice(q * LANES, (q + 1) * LANES)
+        normed[:, lanes] = (floats[:, lanes] * scale * gains[q : q + 1, :]).astype(BF16)
 
     to_blocks = one_hot_to_blocks(wide, wide)
     per_block = wide
@@ -121,9 +145,6 @@
             )
         rx[j, ep] = tx[j, ep]
 
-    pl.semaphore_wait(barrier, experts)
-    pl.semaphore_signal(ready_sem, inc=1, device_id={"tp": other}, device_id_type=MESH)
-
     def dispatch(j, offset):
         to = peer(offset)
         return pltpu.make_async_remote_copy(
@@ -131,18 +152,34 @@
             device_id={"ep": to}, device_id_type=MESH,
         )
 
-    for j in range(chunks):
-        for offset in order:
+    @pl.when(c == 0)
+    def _():
+        pl.semaphore_wait(barrier, len(straight))
+        pl.semaphore_signal(lines_sem, inc=1, device_id={"tp": 1}, device_id_type=MESH)
+        for offset in straight:
+            if offset[1]:
+                pl.semaphore_signal(planes_sem, inc=1, device_id={"ep": peer(offset)}, device_id_type=MESH)
+
+    @pl.when(c == 1)
+    def _():
+        pl.semaphore_wait(lines_sem, 1)
+
+    for j in range(chunks):
+        for offset in straight:
             dispatch(j, offset).start()
-    pushes = [
-        pltpu.make_async_remote_copy(
-            src_ref=src.at[0], dst_ref=dst.at[1], send_sem=push_send.at[i], recv_sem=push_recv.at[i],
-            device_id={"tp": other}, device_id_type=MESH,
-        )
-        for i, (src, dst) in enumerate([(gate_hbm, gate), (up_hbm, up), (down_hbm, down)])
-    ]
-    for copy in pushes:
-        copy.start()
+
+    @pl.when(c == 0)
+    def _():
+        pl.semaphore_wait(planes_sem, side - 1)
+        pl.semaphore_signal(lines_sem, inc=1, device_id={"tp": 1}, device_id_type=MESH)
+
+    @pl.when(c == 1)
+    def _():
+        pl.semaphore_wait(lines_sem, 1)
+
+    for j in range(chunks):
+        for offset in diagonal:
+            dispatch(j, offset).start()
 
     def swiglu(inputs, pairs):
         hidden = []
@@ -167,15 +204,17 @@
     small[3].wait()
     small[4].wait()
     weights = weight[...]
-    weight_at = functools.reduce(
-        jnp.add, [jnp.where(hit, weights[:, k : k + 1], 0.0) for k, hit in enumerate(hits)]
-    )
-    high = weight_at.astype(BF16)
-    low = (weight_at - high.astype(F32)).astype(BF16)
+    weight_t = functools.reduce(jnp.add, [jnp.where(hit, weights[k : k + 1, :], 0.0) for k, hit in enumerate(hits)])
+    high = weight_t.astype(BF16)
+    low = (weight_t - high.astype(F32)).astype(BF16)
+    eye = (iota((local_tokens, local_tokens), 0) == iota((local_tokens, local_tokens), 1)).astype(F32).astype(BF16)
+    turned = [
+        lax.dot_general(eye, part, (((1,), (1,)), ((), ())), preferred_element_type=F32).astype(BF16)
+        for part in (high, low, rank_t.astype(BF16))
+    ]
     columns = experts * cores * thin
-    col = iota((LANES, columns), 1)
-    expand = (iota((LANES, columns), 0) == col // (cores * thin)).astype(F32).astype(BF16)
-    spread = dot(jnp.concatenate([high, low, rank_b], axis=0), expand)
+    expand = (iota((experts, columns), 0) == iota((experts, columns), 1) // (cores * thin)).astype(F32).astype(BF16)
+    spread = dot(jnp.concatenate(turned, axis=0), expand)
     col = iota((local_tokens, columns), 1)
     slot_base = ((col // thin) % cores * chunks).astype(F32)
     q_col = col % thin
@@ -198,7 +237,6 @@
         copy.wait()
     for copy in pushes:
         copy.wait()
-    pl.semaphore_wait(ready_sem, 1)
 
     to_rows = one_hot_to_rows(wide, wide)
     per_back = 2 * LANES // thin
@@ -265,10 +303,10 @@
         pltpu.make_async_copy(sent, sent, send2_sem.at[j]).wait()
     pair.wait()
     scale = lax.rsqrt((mine + sq_recv[...]) / width + EPSILON)
-    gain = out_gain[...].astype(F32)
+    gains = out_gain[...].astype(F32)
     for q in range(thin):
         lanes = slice(q * LANES, (q + 1) * LANES)
-        out_ref[:, lanes] = (total[q * local_tokens : (q + 1) * local_tokens] * scale * gain[:, lanes]).astype(BF16)
+        out_ref[:, lanes] = (total[q * local_tokens : (q + 1) * local_tokens] * scale * gains[q : q + 1, :]).astype(BF16)
 
 
 def body(tokens, in_gain, route_expert, route_weight, gate_weight, up_weight, down_weight, shared_gate, shared_up, shared_down, out_gain):
@@ -283,8 +321,8 @@
     any_spec = pl.BlockSpec(memory_space=pl.ANY)
     vmem, dma = pltpu.VMEM, pltpu.SemaphoreType.DMA
     scratch = [
-        vmem((local_tokens, width), BF16), vmem((1, width), BF16), vmem((local_tokens, top_count), jnp.int32),
-        vmem((local_tokens, top_count), F32), vmem((1, half), BF16),
+        vmem((local_tokens, width), BF16), vmem((wide, LANES), BF16), vmem((top_count, local_tokens), jnp.int32),
+        vmem((top_count, local_tokens), F32), vmem((thin, LANES), BF16),
         vmem((cores, width, hidden), BF16), vmem((cores, width, hidden), BF16), vmem((cores, hidden, width), BF16),
         vmem((width, hidden), BF16), vmem((width, hidden), BF16), vmem((hidden, width), BF16),
         vmem((local_tokens, width), BF16),
@@ -295,7 +333,7 @@
         vmem((cores, local_tokens, half), BF16), vmem((local_tokens, half), BF16), vmem((thin * local_tokens, LANES), F32),
         vmem((local_tokens, LANES), F32), vmem((local_tokens, LANES), F32),
         dma((5,)), dma((6,)), dma((3,)), dma((3,)), dma((chunks,)), dma((chunks,)), dma((chunks,)), dma((chunks,)),
-        dma((2,)), dma((2,)), pltpu.SemaphoreType.REGULAR,
+        dma((2,)), dma((2,)), pltpu.SemaphoreType.REGULAR, pltpu.SemaphoreType.REGULAR, pltpu.SemaphoreType.REGULAR,
     ]
     return pl.pallas_call(
         functools.partial(kernel, experts, cores, slots),
@@ -305,8 +343,8 @@
         scratch_shapes=scratch,
         compiler_params=pltpu.CompilerParams(collective_id=0, has_side_effects=True, vmem_limit_bytes=60 * 1024 * 1024),
     )(
-        tokens, in_gain.reshape(1, width), route_expert, route_weight, gate_weight, up_weight, down_weight,
-        shared_gate, shared_up, shared_down, out_gain.reshape(1, half),
+        tokens, in_gain.reshape(wide, LANES), route_expert.T, route_weight.T, gate_weight, up_weight, down_weight,
+        shared_gate, shared_up, shared_down, out_gain.reshape(thin, LANES),
     )
 
 

time: 61.8 us -> 56.9 us (0.921)
  local copies, waits for them, and re-layouts: 6.78 us -> 1.47 us
    unnamed x3 -> x1, local copies, waits for them, and re-layouts: 4.21 us -> 1.47 us
    reshape x2 -> x0, local copies, waits for them, and re-layouts: 2.57 us -> none  [the longest x1 1.29 us: body(): in_gain.reshape(1, width)]
where the time goes in v2:
time: 56.9 us; the launch traced here: 56.7 us
  Pallas kernels  55.3 us (97%)
  local copies, waits for them, and re-layouts  1.47 us (3%)
    pallas_call x1, Pallas kernels, body(): pl.pallas_call(functools.partial(kernel, experts, cores, slots), out_shap...  55.3 us
    unnamed x1, local copies, waits for them, and re-layouts  1.47 us

profile of v2, /device:TPU:513, one launch (start us, length us, event | category | flops | bytes accessed | tf_op | source)
XLA Modules:
  0.0 56.7 jit_solution(16039292747770414494)
XLA Ops:
  0.0 55.3 %shard_map.109 = bf16[32,1024]{1,0:T(8,128)(2,1)} custom-call(bf16[32,2048]{1,0:T(8,128)(2,1)} %tokens_hbm.1, bf16[16,128]{1,0:T(8,128)(2,1)} %bitcast.4, s32[6,32]{1,0:T(8,128)} %bitcast.5, f32[6,32]{1,0:T(8,128)} %bitcast.6, bf16[1,2048,384]{2,1,0:T(8,128)(2,1)} %gate_hbm.1, bf16[1,2048,384]{2,1,0:T(8,128)(2,1)} %up_hbm.1, bf16[1,384,2048]{2,1,0:T(8,128)(2,1)} %down_hbm.1, ...), custom_call_target="tpu_custom_call" | custom-call | tf_op jit(solution)/shard_map/pallas_call | solution.py:338
  55.3 1.5 %copy.13 = bf16[32,1024]{1,0:T(8,128)(2,1)} copy(bf16[32,1024]{1,0:T(8,128)(2,1)} %shard_map.109) | data formatting | bytes 131072

commit v3 on v2

--- a/solution.py
+++ b/solution.py
@@ -20,9 +20,7 @@
         return min(step, side - step)
 
     offsets = [(dx, dy) for dy in range(side) for dx in range(side) if dx or dy]
-    offsets = sorted(offsets, key=lambda o: -(reach(o[0]) + reach(o[1])))
-    straight = [o for o in offsets if not (o[0] and o[1])]
-    return straight, [o for o in offsets if o[0] and o[1]]
+    return sorted(offsets, key=lambda o: -(reach(o[0]) + reach(o[1])))
 
 
 def dot(a, b):
@@ -51,7 +49,7 @@
     out_ref,
     tokens, in_gain, route, weight, out_gain, gate, up, down, sgate, sup, sdown,
     normed, tx, rx, rows, tx2, rx2, picks, shared_send, shared_recv, shared_half, sq_send, sq_recv,
-    small_sem, weight_sem, push_send, push_recv, send_sem, recv_sem, send2_sem, recv2_sem, pair_send, pair_recv, pair_sem, lines_sem, planes_sem,
+    small_sem, weight_sem, push_send, push_recv, send_sem, recv_sem, send2_sem, recv2_sem, pair_send, pair_recv, pair_sem,
 ):
     ep, c = lax.axis_index("ep"), lax.axis_index("tp")
     other = 1 - c
@@ -62,8 +60,7 @@
     chunks = slots // cores
     wide = width // LANES
     thin = half // LANES
-    straight, diagonal = far_first(side)
-    order = diagonal + straight
+    order = far_first(side)
 
     def peer(offset):
         return lax.rem(here_y + offset[1], side) * side + lax.rem(here_x + offset[0], side)
@@ -78,30 +75,9 @@
         copy.start()
     barrier = pltpu.get_barrier_semaphore()
 
-    @pl.when(c == 0)
-    def _():
-        pl.semaphore_signal(barrier, inc=1, device_id={"tp": 1}, device_id_type=MESH)
-
-    @pl.when(c == 1)
-    def _():
-        pl.semaphore_wait(barrier, 1)
-        pl.semaphore_signal(pair_sem, inc=1, device_id={"tp": 0}, device_id_type=MESH)
-
-    @pl.when(c == 0)
-    def _():
-        pl.semaphore_wait(pair_sem, 1)
-        for offset in straight:
-            pl.semaphore_signal(barrier, inc=1, device_id={"ep": peer(offset)}, device_id_type=MESH)
-
-    pushes = [
-        pltpu.make_async_remote_copy(
-            src_ref=src.at[0], dst_ref=dst.at[1], send_sem=push_send.at[i], recv_sem=push_recv.at[i],
-            device_id={"tp": other}, device_id_type=MESH,
-        )
-        for i, (src, dst) in enumerate([(gate_hbm, gate), (up_hbm, up), (down_hbm, down)])
-    ]
-    for copy in pushes:
-        copy.start()
+    for offset in order:
+        pl.semaphore_signal(barrier, inc=1, device_id={"ep": peer(offset)}, device_id_type=MESH)
+    pl.semaphore_signal(barrier, inc=1, device_id={"tp": other}, device_id_type=MESH)
     loads = [
         pltpu.make_async_copy(src, dst, weight_sem.at[i])
         for i, (src, dst) in enumerate(
@@ -145,41 +121,41 @@
             )
         rx[j, ep] = tx[j, ep]
 
-    def dispatch(j, offset):
-        to = peer(offset)
+    def dispatch(j, to):
         return pltpu.make_async_remote_copy(
             src_ref=tx.at[j, to], dst_ref=rx.at[j, ep], send_sem=send_sem.at[j], recv_sem=recv_sem.at[j],
             device_id={"ep": to}, device_id_type=MESH,
         )
 
+    pushes = [
+        pltpu.make_async_remote_copy(
+            src_ref=src.at[0], dst_ref=dst.at[1], send_sem=push_send.at[i], recv_sem=push_recv.at[i],
+            device_id={"tp": other}, device_id_type=MESH,
+        )
+        for i, (src, dst) in enumerate([(gate_hbm, gate), (up_hbm, up), (down_hbm, down)])
+    ]
+
+    @pl.when(c == 1)
+    def _():
+        pl.semaphore_wait(barrier, experts)
+        pl.semaphore_signal(pair_sem, inc=1, device_id={"tp": 0}, device_id_type=MESH)
+
     @pl.when(c == 0)
     def _():
-        pl.semaphore_wait(barrier, len(straight))
-        pl.semaphore_signal(lines_sem, inc=1, device_id={"tp": 1}, device_id_type=MESH)
-        for offset in straight:
-            if offset[1]:
-                pl.semaphore_signal(planes_sem, inc=1, device_id={"ep": peer(offset)}, device_id_type=MESH)
+        pl.semaphore_wait(pair_sem, 1)
+        for copy in pushes:
+            copy.start()
+        pl.semaphore_wait(barrier, experts)
+        pl.semaphore_signal(pair_sem, inc=1, device_id={"tp": 1}, device_id_type=MESH)
+
+    for j in range(chunks):
+        for offset in order:
+            dispatch(j, peer(offset)).start()
 
     @pl.when(c == 1)
     def _():
-        pl.semaphore_wait(lines_sem, 1)
-
-    for j in range(chunks):
-        for offset in straight:
-            dispatch(j, offset).start()
-
-    @pl.when(c == 0)
-    def _():
-        pl.semaphore_wait(planes_sem, side - 1)
-        pl.semaphore_signal(lines_sem, inc=1, device_id={"tp": 1}, device_id_type=MESH)
-
-    @pl.when(c == 1)
-    def _():
-        pl.semaphore_wait(lines_sem, 1)
-
-    for j in range(chunks):
-        for offset in diagonal:
-            dispatch(j, offset).start()
+        for copy in pushes:
+            copy.start()
 
     def swiglu(inputs, pairs):
         hidden = []
@@ -272,8 +248,15 @@
                     dot(to_thin, stacked).astype(BF16).reshape(per_back, thin, LANES)
                 )
         for offset in order:
-            for core in range(cores):
-                give_back(j, offset, core).start()
+            give_back(j, offset, c).start()
+        if j == 0:
+
+            @pl.when(c == 1)
+            def _():
+                pl.semaphore_wait(pair_sem, 1)
+
+        for offset in order:
+            give_back(j, offset, other).start()
         back = pltpu.make_async_remote_copy(
             src_ref=tx2.at[j, other, ep], dst_ref=rx2.at[j, ep * cores + c], send_sem=send2_sem.at[j], recv_sem=recv2_sem.at[j],
             device_id={"tp": other}, device_id_type=MESH,
@@ -333,7 +316,7 @@
         vmem((cores, local_tokens, half), BF16), vmem((local_tokens, half), BF16), vmem((thin * local_tokens, LANES), F32),
         vmem((local_tokens, LANES), F32), vmem((local_tokens, LANES), F32),
         dma((5,)), dma((6,)), dma((3,)), dma((3,)), dma((chunks,)), dma((chunks,)), dma((chunks,)), dma((chunks,)),
-        dma((2,)), dma((2,)), pltpu.SemaphoreType.REGULAR, pltpu.SemaphoreType.REGULAR, pltpu.SemaphoreType.REGULAR,
+        dma((2,)), dma((2,)), pltpu.SemaphoreType.REGULAR,
     ]
     return pl.pallas_call(
         functools.partial(kernel, experts, cores, slots),

time: 56.9 us -> 53 us (0.931)
  Pallas kernels: 55.3 us -> 51.3 us
    pallas_call x1, Pallas kernels: 55.3 us -> 51.3 us  [body(): pl.pallas_call(functools.partial(kernel, experts, cores, slots), out_shap...]
where the time goes in v3:
time: 53 us; the launch traced here: 52.8 us
  Pallas kernels  51.3 us (97%)
  local copies, waits for them, and re-layouts  1.47 us (3%)
    pallas_call x1, Pallas kernels, body(): pl.pallas_call(functools.partial(kernel, experts, cores, slots), out_shap...  51.3 us
    unnamed x1, local copies, waits for them, and re-layouts  1.47 us

profile of v3, /device:TPU:513, one launch (start us, length us, event | category | flops | bytes accessed | tf_op | source)
XLA Modules:
  0.0 52.8 jit_solution(49913091987646749)
XLA Ops:
  0.0 51.3 %shard_map.109 = bf16[32,1024]{1,0:T(8,128)(2,1)} custom-call(bf16[32,2048]{1,0:T(8,128)(2,1)} %tokens_hbm.1, bf16[16,128]{1,0:T(8,128)(2,1)} %bitcast.4, s32[6,32]{1,0:T(8,128)} %bitcast.5, f32[6,32]{1,0:T(8,128)} %bitcast.6, bf16[1,2048,384]{2,1,0:T(8,128)(2,1)} %gate_hbm.1, bf16[1,2048,384]{2,1,0:T(8,128)(2,1)} %up_hbm.1, bf16[1,384,2048]{2,1,0:T(8,128)(2,1)} %down_hbm.1, ...), custom_call_target="tpu_custom_call" | custom-call | tf_op jit(solution)/shard_map/pallas_call | solution.py:321
  51.3 1.5 %copy.13 = bf16[32,1024]{1,0:T(8,128)(2,1)} copy(bf16[32,1024]{1,0:T(8,128)(2,1)} %shard_map.109) | data formatting | bytes 131072

commit v4 on v3

--- a/solution.py
+++ b/solution.py
@@ -61,6 +61,8 @@
     wide = width // LANES
     thin = half // LANES
     order = far_first(side)
+    is_root = ep == 0
+    counts_partner = is_root == (c == 0)
 
     def peer(offset):
         return lax.rem(here_y + offset[1], side) * side + lax.rem(here_x + offset[0], side)
@@ -77,7 +79,11 @@
 
     for offset in order:
         pl.semaphore_signal(barrier, inc=1, device_id={"ep": peer(offset)}, device_id_type=MESH)
-    pl.semaphore_signal(barrier, inc=1, device_id={"tp": other}, device_id_type=MESH)
+
+    @pl.when(jnp.logical_not(counts_partner))
+    def _():
+        pl.semaphore_signal(barrier, inc=1, device_id={"tp": other}, device_id_type=MESH)
+
     loads = [
         pltpu.make_async_copy(src, dst, weight_sem.at[i])
         for i, (src, dst) in enumerate(
@@ -135,27 +141,47 @@
         for i, (src, dst) in enumerate([(gate_hbm, gate), (up_hbm, up), (down_hbm, down)])
     ]
 
-    @pl.when(c == 1)
-    def _():
-        pl.semaphore_wait(barrier, experts)
-        pl.semaphore_signal(pair_sem, inc=1, device_id={"tp": 0}, device_id_type=MESH)
-
-    @pl.when(c == 0)
-    def _():
-        pl.semaphore_wait(pair_sem, 1)
+    def tell_partner():
+        pl.semaphore_signal(pair_sem, inc=1, device_id={"tp": other}, device_id_type=MESH)
+
+    def push():
         for copy in pushes:
             copy.start()
+
+    @pl.when(jnp.logical_and(c == 0, is_root))
+    def _():
         pl.semaphore_wait(barrier, experts)
-        pl.semaphore_signal(pair_sem, inc=1, device_id={"tp": 1}, device_id_type=MESH)
+        tell_partner()
+        push()
+
+    @pl.when(jnp.logical_and(c == 0, jnp.logical_not(is_root)))
+    def _():
+        pl.semaphore_wait(pair_sem, 1)
+        push()
+        pl.semaphore_wait(barrier, experts - 1)
+        tell_partner()
+
+    @pl.when(jnp.logical_and(c == 1, is_root))
+    def _():
+        pl.semaphore_wait(barrier, experts - 1)
+
+    @pl.when(jnp.logical_and(c == 1, jnp.logical_not(is_root)))
+    def _():
+        pl.semaphore_wait(barrier, experts)
+        tell_partner()
 
     for j in range(chunks):
         for offset in order:
             dispatch(j, peer(offset)).start()
 
+    @pl.when(jnp.logical_and(c == 1, is_root))
+    def _():
+        pl.semaphore_wait(pair_sem, 1)
+        tell_partner()
+
     @pl.when(c == 1)
     def _():
-        for copy in pushes:
-            copy.start()
+        push()
 
     def swiglu(inputs, pairs):
         hidden = []
@@ -225,7 +251,15 @@
             device_id={"ep": to, "tp": core}, device_id_type=MESH,
         )
 
-    partner_back = []
+    def to_other_plane(j):
+        for offset in order:
+            give_back(j, offset, other).start()
+        back = pltpu.make_async_remote_copy(
+            src_ref=tx2.at[j, other, ep], dst_ref=rx2.at[j, ep * cores + c], send_sem=send2_sem.at[j], recv_sem=recv2_sem.at[j],
+            device_id={"tp": other}, device_id_type=MESH,
+        )
+        back.start()
+
     for j in range(chunks):
         arrived = rx.at[j, pl.ds(0, experts - 1)]
         pltpu.make_async_copy(arrived, arrived, recv_sem.at[j]).wait()
@@ -249,20 +283,25 @@
                 )
         for offset in order:
             give_back(j, offset, c).start()
+        rx2[j, ep * cores + c] = tx2[j, c, ep]
         if j == 0:
 
-            @pl.when(c == 1)
+            @pl.when(jnp.logical_and(c == 0, is_root))
             def _():
                 pl.semaphore_wait(pair_sem, 1)
 
-        for offset in order:
-            give_back(j, offset, other).start()
-        back = pltpu.make_async_remote_copy(
-            src_ref=tx2.at[j, other, ep], dst_ref=rx2.at[j, ep * cores + c], send_sem=send2_sem.at[j], recv_sem=recv2_sem.at[j],
-            device_id={"tp": other}, device_id_type=MESH,
-        )
-        back.start()
-        rx2[j, ep * cores + c] = tx2[j, c, ep]
+        @pl.when(c == 0)
+        def _():
+            to_other_plane(j)
+
+    @pl.when(jnp.logical_and(c == 1, jnp.logical_not(is_root)))
+    def _():
+        pl.semaphore_wait(pair_sem, 1)
+
+    @pl.when(c == 1)
+    def _():
+        for j in range(chunks):
+            to_other_plane(j)
 
     total = shared_half[...]
     for j in range(chunks):

time: 53 us -> 53.1 us (level)
  no operation moved by 1% of the time
where the time goes in v4:
time: 53.1 us; the launch traced here: 53 us
  Pallas kernels  51.5 us (97%)
  local copies, waits for them, and re-layouts  1.47 us (3%)
    pallas_call x1, Pallas kernels, body(): pl.pallas_call(functools.partial(kernel, experts, cores, slots), out_shap...  51.5 us
    unnamed x1, local copies, waits for them, and re-layouts  1.47 us

profile of v4, /device:TPU:513, one launch (start us, length us, event | category | flops | bytes accessed | tf_op | source)
XLA Modules:
  0.0 53.0 jit_solution(7184761560349544329)
XLA Ops:
  0.0 51.5 %shard_map.109 = bf16[32,1024]{1,0:T(8,128)(2,1)} custom-call(bf16[32,2048]{1,0:T(8,128)(2,1)} %tokens_hbm.1, bf16[16,128]{1,0:T(8,128)(2,1)} %bitcast.4, s32[6,32]{1,0:T(8,128)} %bitcast.5, f32[6,32]{1,0:T(8,128)} %bitcast.6, bf16[1,2048,384]{2,1,0:T(8,128)(2,1)} %gate_hbm.1, bf16[1,2048,384]{2,1,0:T(8,128)(2,1)} %up_hbm.1, bf16[1,384,2048]{2,1,0:T(8,128)(2,1)} %down_hbm.1, ...), custom_call_target="tpu_custom_call" | custom-call | tf_op jit(solution)/shard_map/pallas_call | solution.py:360
  51.5 1.5 %copy.13 = bf16[32,1024]{1,0:T(8,128)(2,1)} copy(bf16[32,1024]{1,0:T(8,128)(2,1)} %shard_map.109) | data formatting | bytes 131072

commit v5 on v4

--- a/solution.py
+++ b/solution.py
@@ -49,7 +49,7 @@
     out_ref,
     tokens, in_gain, route, weight, out_gain, gate, up, down, sgate, sup, sdown,
     normed, tx, rx, rows, tx2, rx2, picks, shared_send, shared_recv, shared_half, sq_send, sq_recv,
-    small_sem, weight_sem, push_send, push_recv, send_sem, recv_sem, send2_sem, recv2_sem, pair_send, pair_recv, pair_sem,
+    small_sem, weight_sem, push_send, push_recv, send_sem, recv_sem, send2_sem, recv2_sem, forward_sem, pair_send, pair_recv, pair_sem, late_sem,
 ):
     ep, c = lax.axis_index("ep"), lax.axis_index("tp")
     other = 1 - c
@@ -62,6 +62,8 @@
     thin = half // LANES
     order = far_first(side)
     is_root = ep == 0
+    is_late = jnp.logical_and(is_root, c == 0)
+    is_mailbox = jnp.logical_and(is_root, c == 1)
     counts_partner = is_root == (c == 0)
 
     def peer(offset):
@@ -77,8 +79,10 @@
         copy.start()
     barrier = pltpu.get_barrier_semaphore()
 
-    for offset in order:
-        pl.semaphore_signal(barrier, inc=1, device_id={"ep": peer(offset)}, device_id_type=MESH)
+    @pl.when(jnp.logical_not(is_late))
+    def _():
+        for offset in order:
+            pl.semaphore_signal(barrier, inc=1, device_id={"ep": peer(offset)}, device_id_type=MESH)
 
     @pl.when(jnp.logical_not(counts_partner))
     def _():
@@ -128,10 +132,19 @@
         rx[j, ep] = tx[j, ep]
 
     def dispatch(j, to):
+        redirect = jnp.logical_and(to == 0, c == 0).astype(jnp.int32)
         return pltpu.make_async_remote_copy(
-            src_ref=tx.at[j, to], dst_ref=rx.at[j, ep], send_sem=send_sem.at[j], recv_sem=recv_sem.at[j],
-            device_id={"ep": to}, device_id_type=MESH,
-        )
+            src_ref=tx.at[j, to], dst_ref=rx.at[j, ep + redirect * experts], send_sem=send_sem.at[j],
+            recv_sem=recv_sem.at[j + redirect * chunks], device_id={"ep": to, "tp": c + redirect}, device_id_type=MESH,
+        )
+
+    forwards = [
+        pltpu.make_async_remote_copy(
+            src_ref=rx.at[j, pl.ds(experts + 1, experts - 1)], dst_ref=rx.at[j, pl.ds(1, experts - 1)],
+            send_sem=forward_sem.at[j], recv_sem=recv_sem.at[j], device_id={"tp": 0}, device_id_type=MESH,
+        )
+        for j in range(chunks)
+    ]
 
     pushes = [
         pltpu.make_async_remote_copy(
@@ -158,7 +171,7 @@
     def _():
         pl.semaphore_wait(pair_sem, 1)
         push()
-        pl.semaphore_wait(barrier, experts - 1)
+        pl.semaphore_wait(barrier, experts - 2)
         tell_partner()
 
     @pl.when(jnp.logical_and(c == 1, is_root))
@@ -173,6 +186,12 @@
     for j in range(chunks):
         for offset in order:
             dispatch(j, peer(offset)).start()
+        if j == 0:
+
+            @pl.when(is_late)
+            def _():
+                for offset in order:
+                    pl.semaphore_signal(late_sem, inc=1, device_id={"ep": peer(offset)}, device_id_type=MESH)
 
     @pl.when(jnp.logical_and(c == 1, is_root))
     def _():
@@ -235,6 +254,19 @@
         total = shared_send[c][:, lanes].astype(F32) + shared_recv[:, lanes].astype(F32)
         shared_half[pl.ds(q * local_tokens, local_tokens)] = total.astype(BF16).astype(F32)
 
+    @pl.when(jnp.logical_and(c == 0, jnp.logical_not(is_root)))
+    def _():
+        pl.semaphore_wait(late_sem, 1)
+        pl.semaphore_signal(late_sem, inc=1, device_id={"tp": 1}, device_id_type=MESH)
+
+    def forward(j):
+        @pl.when(is_mailbox)
+        def _():
+            arrived = rx.at[j, pl.ds(experts + 1, experts - 1)]
+            pltpu.make_async_copy(arrived, arrived, recv_sem.at[chunks + j]).wait()
+            forwards[j].start()
+
+    forward(0)
     for copy in loads[3:]:
         copy.wait()
     for copy in pushes:
@@ -261,6 +293,8 @@
         back.start()
 
     for j in range(chunks):
+        if j:
+            forward(j)
         arrived = rx.at[j, pl.ds(0, experts - 1)]
         pltpu.make_async_copy(arrived, arrived, recv_sem.at[j]).wait()
         for b in range(experts // per_block):
@@ -286,22 +320,16 @@
         rx2[j, ep * cores + c] = tx2[j, c, ep]
         if j == 0:
 
-            @pl.when(jnp.logical_and(c == 0, is_root))
+            @pl.when(is_late)
             def _():
                 pl.semaphore_wait(pair_sem, 1)
 
-        @pl.when(c == 0)
-        def _():
-            to_other_plane(j)
-
-    @pl.when(jnp.logical_and(c == 1, jnp.logical_not(is_root)))
-    def _():
-        pl.semaphore_wait(pair_sem, 1)
-
-    @pl.when(c == 1)
-    def _():
-        for j in range(chunks):
-            to_other_plane(j)
+            @pl.when(jnp.logical_and(c == 1, jnp.logical_not(is_root)))
+            def _():
+                pl.semaphore_wait(pair_sem, 1)
+                pl.semaphore_wait(late_sem, 1)
+
+        to_other_plane(j)
 
     total = shared_half[...]
     for j in range(chunks):
@@ -323,6 +351,11 @@
         pltpu.make_async_copy(sent, sent, send_sem.at[j]).wait()
         sent = rx2.at[j, pl.ds(0, experts * cores - 1)]
         pltpu.make_async_copy(sent, sent, send2_sem.at[j]).wait()
+    @pl.when(is_mailbox)
+    def _():
+        for copy in forwards:
+            copy.wait_send()
+
     pair.wait()
     scale = lax.rsqrt((mine + sq_recv[...]) / width + EPSILON)
     gains = out_gain[...].astype(F32)
@@ -348,14 +381,14 @@
         vmem((cores, width, hidden), BF16), vmem((cores, width, hidden), BF16), vmem((cores, hidden, width), BF16),
         vmem((width, hidden), BF16), vmem((width, hidden), BF16), vmem((hidden, width), BF16),
         vmem((local_tokens, width), BF16),
-        vmem((chunks, experts, wide, LANES), BF16), vmem((chunks, experts, wide, LANES), BF16),
+        vmem((chunks, experts, wide, LANES), BF16), vmem((chunks, 2 * experts, wide, LANES), BF16),
         vmem((experts, width), BF16),
         vmem((chunks, cores, experts, thin, LANES), BF16), vmem((chunks, experts * cores, thin, LANES), BF16),
         vmem((chunks, 2 * thin * local_tokens, experts * cores * thin), BF16),
         vmem((cores, local_tokens, half), BF16), vmem((local_tokens, half), BF16), vmem((thin * local_tokens, LANES), F32),
         vmem((local_tokens, LANES), F32), vmem((local_tokens, LANES), F32),
-        dma((5,)), dma((6,)), dma((3,)), dma((3,)), dma((chunks,)), dma((chunks,)), dma((chunks,)), dma((chunks,)),
-        dma((2,)), dma((2,)), pltpu.SemaphoreType.REGULAR,
+        dma((5,)), dma((6,)), dma((3,)), dma((3,)), dma((chunks,)), dma((2 * chunks,)), dma((chunks,)), dma((chunks,)),
+        dma((chunks,)), dma((2,)), dma((2,)), pltpu.SemaphoreType.REGULAR, pltpu.SemaphoreType.REGULAR,
     ]
     return pl.pallas_call(
         functools.partial(kernel, experts, cores, slots),

time: 53.1 us -> 51.7 us (0.974)
  Pallas kernels: 51.5 us -> 50.1 us
    pallas_call x1, Pallas kernels: 51.5 us -> 50.1 us  [body(): pl.pallas_call(functools.partial(kernel, experts, cores, slots), out_shap...]
where the time goes in v5:
time: 51.7 us; the launch traced here: 51.6 us
  Pallas kernels  50.1 us (97%)
  local copies, waits for them, and re-layouts  1.47 us (3%)
    pallas_call x1, Pallas kernels, body(): pl.pallas_call(functools.partial(kernel, experts, cores, slots), out_shap...  50.1 us
    unnamed x1, local copies, waits for them, and re-layouts  1.47 us

profile of v5, /device:TPU:513, one launch (start us, length us, event | category | flops | bytes accessed | tf_op | source)
XLA Modules:
  0.0 51.6 jit_solution(9694272971551197555)
XLA Ops:
  0.0 50.1 %shard_map.109 = bf16[32,1024]{1,0:T(8,128)(2,1)} custom-call(bf16[32,2048]{1,0:T(8,128)(2,1)} %tokens_hbm.1, bf16[16,128]{1,0:T(8,128)(2,1)} %bitcast.4, s32[6,32]{1,0:T(8,128)} %bitcast.5, f32[6,32]{1,0:T(8,128)} %bitcast.6, bf16[1,2048,384]{2,1,0:T(8,128)(2,1)} %gate_hbm.1, bf16[1,2048,384]{2,1,0:T(8,128)(2,1)} %up_hbm.1, bf16[1,384,2048]{2,1,0:T(8,128)(2,1)} %down_hbm.1, ...), custom_call_target="tpu_custom_call" | custom-call | tf_op jit(solution)/shard_map/pallas_call | solution.py:393
  50.1 1.5 %copy.13 = bf16[32,1024]{1,0:T(8,128)(2,1)} copy(bf16[32,1024]{1,0:T(8,128)(2,1)} %shard_map.109) | data formatting | bytes 131072

commit v6 on v5

--- a/solution.py
+++ b/solution.py
@@ -88,6 +88,27 @@
     def _():
         pl.semaphore_signal(barrier, inc=1, device_id={"tp": other}, device_id_type=MESH)
 
+    pushes = [
+        pltpu.make_async_remote_copy(
+            src_ref=src.at[0], dst_ref=dst.at[1], send_sem=push_send.at[i], recv_sem=push_recv.at[i],
+            device_id={"tp": other}, device_id_type=MESH,
+        )
+        for i, (src, dst) in enumerate([(gate_hbm, gate), (up_hbm, up), (down_hbm, down)])
+    ]
+
+    def tell_partner():
+        pl.semaphore_signal(pair_sem, inc=1, device_id={"tp": other}, device_id_type=MESH)
+
+    def push():
+        for copy in pushes:
+            copy.start()
+
+    @pl.when(jnp.logical_and(c == 0, is_root))
+    def _():
+        pl.semaphore_wait(barrier, experts)
+        tell_partner()
+        push()
+
     loads = [
         pltpu.make_async_copy(src, dst, weight_sem.at[i])
         for i, (src, dst) in enumerate(
@@ -146,31 +167,9 @@
         for j in range(chunks)
     ]
 
-    pushes = [
-        pltpu.make_async_remote_copy(
-            src_ref=src.at[0], dst_ref=dst.at[1], send_sem=push_send.at[i], recv_sem=push_recv.at[i],
-            device_id={"tp": other}, device_id_type=MESH,
-        )
-        for i, (src, dst) in enumerate([(gate_hbm, gate), (up_hbm, up), (down_hbm, down)])
-    ]
-
-    def tell_partner():
-        pl.semaphore_signal(pair_sem, inc=1, device_id={"tp": other}, device_id_type=MESH)
-
-    def push():
-        for copy in pushes:
-            copy.start()
-
-    @pl.when(jnp.logical_and(c == 0, is_root))
-    def _():
-        pl.semaphore_wait(barrier, experts)
-        tell_partner()
-        push()
-
     @pl.when(jnp.logical_and(c == 0, jnp.logical_not(is_root)))
     def _():
         pl.semaphore_wait(pair_sem, 1)
-        push()
         pl.semaphore_wait(barrier, experts - 2)
         tell_partner()
 
@@ -198,7 +197,7 @@
         pl.semaphore_wait(pair_sem, 1)
         tell_partner()
 
-    @pl.when(c == 1)
+    @pl.when(jnp.logical_not(is_late))
     def _():
         push()
 

time: 51.7 us -> 51.4 us (level)
  no operation moved by 1% of the time
where the time goes in v6:
time: 51.4 us; the launch traced here: 51.3 us
  Pallas kernels  49.8 us (97%)
  local copies, waits for them, and re-layouts  1.47 us (3%)
    pallas_call x1, Pallas kernels, body(): pl.pallas_call(functools.partial(kernel, experts, cores, slots), out_shap...  49.8 us
    unnamed x1, local copies, waits for them, and re-layouts  1.47 us

profile of v6, /device:TPU:513, one launch (start us, length us, event | category | flops | bytes accessed | tf_op | source)
XLA Modules:
  0.0 51.3 jit_solution(12270789361815830265)
XLA Ops:
  0.0 49.8 %shard_map.109 = bf16[32,1024]{1,0:T(8,128)(2,1)} custom-call(bf16[32,2048]{1,0:T(8,128)(2,1)} %tokens_hbm.1, bf16[16,128]{1,0:T(8,128)(2,1)} %bitcast.4, s32[6,32]{1,0:T(8,128)} %bitcast.5, f32[6,32]{1,0:T(8,128)} %bitcast.6, bf16[1,2048,384]{2,1,0:T(8,128)(2,1)} %gate_hbm.1, bf16[1,2048,384]{2,1,0:T(8,128)(2,1)} %up_hbm.1, bf16[1,384,2048]{2,1,0:T(8,128)(2,1)} %down_hbm.1, ...), custom_call_target="tpu_custom_call" | custom-call | tf_op jit(solution)/shard_map/pallas_call | solution.py:392
  49.8 1.5 %copy.13 = bf16[32,1024]{1,0:T(8,128)(2,1)} copy(bf16[32,1024]{1,0:T(8,128)(2,1)} %shard_map.109) | data formatting | bytes 131072

commit v7 on v6

--- a/solution.py
+++ b/solution.py
@@ -247,17 +247,6 @@
                     q_col == q, value, 0.0
                 ).astype(BF16)
 
-    pair.wait()
-    for q in range(thin):
-        lanes = slice(q * LANES, (q + 1) * LANES)
-        total = shared_send[c][:, lanes].astype(F32) + shared_recv[:, lanes].astype(F32)
-        shared_half[pl.ds(q * local_tokens, local_tokens)] = total.astype(BF16).astype(F32)
-
-    @pl.when(jnp.logical_and(c == 0, jnp.logical_not(is_root)))
-    def _():
-        pl.semaphore_wait(late_sem, 1)
-        pl.semaphore_signal(late_sem, inc=1, device_id={"tp": 1}, device_id_type=MESH)
-
     def forward(j):
         @pl.when(is_mailbox)
         def _():
@@ -266,9 +255,20 @@
             forwards[j].start()
 
     forward(0)
+    pair.wait()
+    for q in range(thin):
+        lanes = slice(q * LANES, (q + 1) * LANES)
+        total = shared_send[c][:, lanes].astype(F32) + shared_recv[:, lanes].astype(F32)
+        shared_half[pl.ds(q * local_tokens, local_tokens)] = total.astype(BF16).astype(F32)
+
+    @pl.when(jnp.logical_and(c == 0, jnp.logical_not(is_root)))
+    def _():
+        pl.semaphore_wait(late_sem, 1)
+        pl.semaphore_signal(late_sem, inc=1, device_id={"tp": 1}, device_id_type=MESH)
+
     for copy in loads[3:]:
         copy.wait()
-    for copy in pushes:
+    for copy in pushes[:2]:
         copy.wait()
 
     to_rows = one_hot_to_rows(wide, wide)
@@ -282,18 +282,13 @@
             device_id={"ep": to, "tp": core}, device_id_type=MESH,
         )
 
-    def to_other_plane(j):
-        for offset in order:
-            give_back(j, offset, other).start()
-        back = pltpu.make_async_remote_copy(
+    def to_partner(j):
+        pltpu.make_async_remote_copy(
             src_ref=tx2.at[j, other, ep], dst_ref=rx2.at[j, ep * cores + c], send_sem=send2_sem.at[j], recv_sem=recv2_sem.at[j],
             device_id={"tp": other}, device_id_type=MESH,
-        )
-        back.start()
-
-    for j in range(chunks):
-        if j:
-            forward(j)
+        ).start()
+
+    for j in range(chunks):
         arrived = rx.at[j, pl.ds(0, experts - 1)]
         pltpu.make_async_copy(arrived, arrived, recv_sem.at[j]).wait()
         for b in range(experts // per_block):
@@ -304,6 +299,8 @@
                     q * per_block : (q + 1) * per_block
                 ]
         hidden = swiglu(rows[...], [(gate[h], up[h]) for h in range(cores)])
+        if j == 0:
+            pushes[2].wait()
         result = functools.reduce(jnp.add, [dot(hidden[h], down[h]) for h in range(cores)]).astype(BF16)
         for b in range(experts // per_back):
             part = result[b * per_back : (b + 1) * per_back]
@@ -314,10 +311,12 @@
                 tx2[j, core, pl.ds(b * per_back, per_back)] = (
                     dot(to_thin, stacked).astype(BF16).reshape(per_back, thin, LANES)
                 )
-        for offset in order:
-            give_back(j, offset, c).start()
         rx2[j, ep * cores + c] = tx2[j, c, ep]
+        if j + 1 < chunks:
+            forward(j + 1)
         if j == 0:
+            for offset in order:
+                give_back(j, offset, c).start()
 
             @pl.when(is_late)
             def _():
@@ -328,7 +327,13 @@
                 pl.semaphore_wait(pair_sem, 1)
                 pl.semaphore_wait(late_sem, 1)
 
-        to_other_plane(j)
+            for offset in order:
+                give_back(j, offset, other).start()
+        else:
+            for offset in order:
+                give_back(j, offset, c).start()
+                give_back(j, offset, other).start()
+        to_partner(j)
 
     total = shared_half[...]
     for j in range(chunks):

time: 51.4 us -> 51.6 us (level)
  no operation moved by 1% of the time
where the time goes in v7:
time: 51.6 us; the launch traced here: 51.5 us
  Pallas kernels  50 us (97%)
  local copies, waits for them, and re-layouts  1.47 us (3%)
    pallas_call x1, Pallas kernels, body(): pl.pallas_call(functools.partial(kernel, experts, cores, slots), out_shap...  50 us
    unnamed x1, local copies, waits for them, and re-layouts  1.47 us

profile of v7, /device:TPU:513, one launch (start us, length us, event | category | flops | bytes accessed | tf_op | source)
XLA Modules:
  0.0 51.5 jit_solution(14724177215546353598)
XLA Ops:
  0.0 50.0 %shard_map.109 = bf16[32,1024]{1,0:T(8,128)(2,1)} custom-call(bf16[32,2048]{1,0:T(8,128)(2,1)} %tokens_hbm.1, bf16[16,128]{1,0:T(8,128)(2,1)} %bitcast.4, s32[6,32]{1,0:T(8,128)} %bitcast.5, f32[6,32]{1,0:T(8,128)} %bitcast.6, bf16[1,2048,384]{2,1,0:T(8,128)(2,1)} %gate_hbm.1, bf16[1,2048,384]{2,1,0:T(8,128)(2,1)} %up_hbm.1, bf16[1,384,2048]{2,1,0:T(8,128)(2,1)} %down_hbm.1, ...), custom_call_target="tpu_custom_call" | custom-call | tf_op jit(solution)/shard_map/pallas_call | solution.py:397
  50.0 1.5 %copy.13 = bf16[32,1024]{1,0:T(8,128)(2,1)} copy(bf16[32,1024]{1,0:T(8,128)(2,1)} %shard_map.109) | data formatting | bytes 131072

commit v8 on v6

--- a/solution.py
+++ b/solution.py
@@ -66,8 +66,12 @@
     is_mailbox = jnp.logical_and(is_root, c == 1)
     counts_partner = is_root == (c == 0)
 
+    turn = jnp.where(c == 0, 1, side - 1)
+    columns_at = [lax.rem(here_x + turn * step, side) for step in range(side)]
+    lines_at = [lax.rem(here_y + turn * step, side) * side for step in range(side)]
+
     def peer(offset):
-        return lax.rem(here_y + offset[1], side) * side + lax.rem(here_x + offset[0], side)
+        return lines_at[offset[1]] + columns_at[offset[0]]
 
     small = [
         pltpu.make_async_copy(src, dst, small_sem.at[i])

time: 51.4 us -> 51.6 us (level)
  no operation moved by 1% of the time
where the time goes in v8:
time: 51.6 us; the launch traced here: 51.4 us
  Pallas kernels  49.9 us (97%)
  local copies, waits for them, and re-layouts  1.47 us (3%)
    pallas_call x1, Pallas kernels, body(): pl.pallas_call(functools.partial(kernel, experts, cores, slots), out_shap...  49.9 us
    unnamed x1, local copies, waits for them, and re-layouts  1.47 us

profile of v8, /device:TPU:513, one launch (start us, length us, event | category | flops | bytes accessed | tf_op | source)
XLA Modules:
  0.0 51.4 jit_solution(15200539160623280997)
XLA Ops:
  0.0 49.9 %shard_map.109 = bf16[32,1024]{1,0:T(8,128)(2,1)} custom-call(bf16[32,2048]{1,0:T(8,128)(2,1)} %tokens_hbm.1, bf16[16,128]{1,0:T(8,128)(2,1)} %bitcast.4, s32[6,32]{1,0:T(8,128)} %bitcast.5, f32[6,32]{1,0:T(8,128)} %bitcast.6, bf16[1,2048,384]{2,1,0:T(8,128)(2,1)} %gate_hbm.1, bf16[1,2048,384]{2,1,0:T(8,128)(2,1)} %up_hbm.1, bf16[1,384,2048]{2,1,0:T(8,128)(2,1)} %down_hbm.1, ...), custom_call_target="tpu_custom_call" | custom-call | tf_op jit(solution)/shard_map/pallas_call | solution.py:396
  49.9 1.5 %copy.13 = bf16[32,1024]{1,0:T(8,128)(2,1)} copy(bf16[32,1024]{1,0:T(8,128)(2,1)} %shard_map.109) | data formatting | bytes 131072
